TPU v7x, 32 devices: a whole 2x2x4 slice. The times are simulated.
32 devices in a mesh: sp: 4 (over y, core), dp: 8 (over z, x).
Axes of the slice: x: 2, y: 2, z: 4, core: 2. Of those that a mesh axis runs over, the one named last changes fastest.
Arguments:
- queries: bfloat16 [8, 704, 2048], P('dp', 'sp'), may hold values from -24 to 24, as said below
- keys: bfloat16 [8, 704, 256], P('dp', 'sp'), may hold values from -24 to 24, as said below
- tokens: bfloat16 [8, 704, 2304], P('dp', 'sp'), may hold values from -18 to 18
- w_value: bfloat16 [2304, 256], P('dp'), may hold values from -0.125 to 0.125
- q_gain: float32 [128], replicated, may hold values from 0.5 to 6, as said below
- k_gain: float32 [128], replicated, may hold values from 0.5 to 6, as said below
Outputs:
- attended: bfloat16 [8, 704, 2048], P('dp', 'sp')
Inputs may be any that keep to these rules, and one draw needn't show every extreme that they name: `queries`: real-valued projected query entries. `keys`: real-valued projected key entries. `q_gain`: positive gains. `k_gain`: positive gains.
All inputs are finite; a program needn't handle non-finite values.
Results may differ from a plain program's by a relative error of at most 0.0022.
The roundings to bfloat16 on the way count: a program that leaves them out, or rounds other values in their place, can miss the bound.
Values may be sent and summed in bfloat16 or wider, within the bound.
A program may use at most 64 MiB of HBM per device.

v0:
```python
import math
import jax
import jax.numpy as jnp
from jax import lax
from jax.sharding import PartitionSpec as P

HD = 128
QH = 16
KVH = 2
GRID_W = 64
epsilon = 1e-06


def unit_rms(vectors, scaling):
    return (
        vectors * lax.rsqrt(jnp.mean(vectors * vectors, axis=-1, keepdims=True) + epsilon) * scaling
    )


def rotary(vectors, row_pos, col_pos):
    head_width = vectors.shape[-1]
    half_width = head_width // 2
    quarter = half_width // 2
    frequency = 10000.0 ** (-jnp.arange(quarter, dtype=jnp.float32) * 2.0 / half_width)

    def rotate_half(section, angle_pos):
        angles = angle_pos[:, None, None] * frequency
        cosine = jnp.cos(angles)
        sine_table = jnp.sin(angles)
        leading = section[..., :quarter]
        second = section[..., quarter:]
        return jnp.concatenate(
            [leading * cosine - second * sine_table, second * cosine + leading * sine_table],
            axis=-1,
        )

    return jnp.concatenate(
        [
            rotate_half(vectors[..., :half_width], row_pos),
            rotate_half(vectors[..., half_width:], col_pos),
        ],
        axis=-1,
    )


def attend(query_heads, key_heads, value_heads):
    length, item_count, joined = query_heads.shape
    head_width = key_heads.shape[-1]
    per_copy = joined // head_width
    block_rows = math.gcd(length, 512)
    blocked = query_heads.reshape(
        length // block_rows, block_rows, item_count, per_copy, head_width
    )

    def one_block(query_block):
        scores = jnp.einsum(
            "qnad,knd->naqk", query_block, key_heads, preferred_element_type=jnp.float32
        ) * head_width ** (-0.5)
        highest = jnp.max(scores, axis=-1, keepdims=True)
        weights = jnp.exp(scores - highest)
        probability = (weights / jnp.sum(weights, axis=-1, keepdims=True)).astype(jnp.bfloat16)
        blended = jnp.einsum(
            "naqk,knd->qnad", probability, value_heads, preferred_element_type=jnp.float32
        )
        return blended.astype(jnp.bfloat16).reshape(block_rows, item_count, joined)

    return lax.map(one_block, blocked).reshape(length, item_count, joined)


def per_device(queries, keys, tokens, w_value, q_gain, k_gain):
    tok_rows = tokens.shape[1]
    devices_sp = lax.axis_size("sp")
    copies = max(devices_sp, KVH)
    repeat_count = copies // KVH
    local_copies = copies // devices_sp
    joined = QH // copies * HD
    token_rows = tokens[0]
    value_sum = jnp.dot(
        token_rows,
        lax.all_gather(w_value, "dp", axis=0, tiled=True),
        preferred_element_type=jnp.float32,
    )
    values = value_sum.astype(jnp.bfloat16).reshape(tok_rows, KVH, HD)
    sp_index = lax.axis_index("sp")
    positions = sp_index * tok_rows + jnp.arange(tok_rows, dtype=jnp.int32)
    row_pos = (positions // GRID_W).astype(jnp.float32)
    col_pos = (positions % GRID_W).astype(jnp.float32)
    query_norm = unit_rms(queries[0].astype(jnp.float32).reshape(tok_rows, QH, HD), q_gain)
    query_rot = rotary(query_norm, row_pos, col_pos).astype(jnp.bfloat16)
    key_norm = unit_rms(keys[0].astype(jnp.float32).reshape(tok_rows, KVH, HD), k_gain)
    key_rot = rotary(key_norm, row_pos, col_pos).astype(jnp.bfloat16)
    query_grouped = query_rot.reshape(tok_rows, copies, joined)
    query_local = lax.all_to_all(query_grouped, "sp", split_axis=1, concat_axis=0, tiled=True)
    key_all, value_all = (
        lax.all_gather(key_rot, "sp", axis=0, tiled=True),
        lax.all_gather(values, "sp", axis=0, tiled=True),
    )
    kv_count = max(1, local_copies // repeat_count)
    kv_start = sp_index * local_copies // repeat_count
    key_local = lax.dynamic_slice_in_dim(key_all, kv_start, kv_count, 1)
    value_local = lax.dynamic_slice_in_dim(value_all, kv_start, kv_count, 1)
    attended = attend(query_local, key_local, value_local)
    returned = lax.all_to_all(attended, "sp", split_axis=0, concat_axis=1, tiled=True)
    return returned.reshape(1, tok_rows, QH * HD)


def solution(mesh):
    in_specs = (
        P("dp", "sp", None),
        P("dp", "sp", None),
        P("dp", "sp", None),
        P("dp", None),
        P(),
        P(),
    )
    out_specs = P("dp", "sp", None)
    return jax.shard_map(
        per_device, mesh=mesh, in_specs=in_specs, out_specs=out_specs, check_vma=False
    )
```

profile of v0, /device:TPU:0, one launch (start us, length us, event | category | flops | bytes accessed | tf_op | source)
XLA Modules:
  0.0 100.0 jit_solution(4973666312808731522)
XLA Ops:
  6.5 0.7 all-gather.2.cloned.1.call-update
  7.3 1.3 %convert_bitcast_fusion = f32[22,8,16,128]{3,1,2,0:T(8,128)S(1)} fusion(bf16[1,176,2048]{2,1,0:T(8,128)(2,1)} %param.8), kind=kLoop, calls=%fused_computation.13 | loop fusion | flops 360448 | bytes 2162688
  8.8 0.4 multiply_reduce_fusion
  9.4 0.7 multiply_cosine_fusion.1
  10.2 0.4 multiply_multiply_fusion
  10.6 1.2 %subtract_convert_fusion.1 = (bf16[176,16,32]{2,1,0:T(8,128)(2,1)S(1)}, bf16[176,16,32]{2,1,0:T(8,128)(2,1)S(1)}, bf16[176,16,32]{2,1,0:T(8,128)(2,1)S(1)}, bf16[176,16,32]{2,1,0:T(8,128)(2,1)S(1)}) fusion(f32[176,16,128]{2,1,0:T(8,128)S(1)} %multiply_multiply_fusion, f32[176,32]{1,0:T(8,128)S(1)} %get-tuple-element.83, f32[176,32]{1,0:T(8,128)S(1)} %get-tuple-element.82, ...), kind=kLoop, calls=%fused_computation.17 | loop fusion | flops 1441792 | bytes 2252800 | tf_op jit(solution)/shard_map/convert.6
  11.8 0.9 pad_maximum_fusion
  13.1 1.0 copy.37
  14.1 4.4 %all-to-all-start = ((bf16[176,4,512]{2,0,1:T(8,128)(2,1)}), bf16[176,4,512]{2,0,1:T(8,128)(2,1)S(1)}, u32[]{:S(2)}, u32[]{:S(2)}) async-start(bf16[176,4,512]{2,0,1:T(8,128)(2,1)} %copy.37), calls=%async_computation | async-start | bytes 1441792 | tf_op jit(solution)/shard_map/all_to_all | solution.py:93
  19.1 0.6 subtract_convert_fusion.3
  19.8 0.6 pad_maximum_fusion.1
  20.3 11.8 %all_gather.9 = bf16[704,2,128]{2,1,0:T(2,128)(2,1)S(1)} all-gather(bf16[176,2,128]{2,1,0:T(2,128)(2,1)S(1)} %pad_maximum_fusion.1), channel_id=1, replica_groups=mesh['sp'=4,'dp'=8] {'sp'}, dimensions={0}, use_global_device_ids=true | all-gather | bytes 450560 | tf_op jit(solution)/shard_map/all_gather | solution.py:95
  32.8 20.6 %all-gather.2.cloned.1.call-done = bf16[2304,256]{1,0:T(8,128)(2,1)} async-done(((bf16[288,256]{1,0:T(8,128)(2,1)}), bf16[2304,256]{1,0:T(8,128)(2,1)}) %all-gather.2.cloned.1.call-update) | async-done | bytes 1179664 | tf_op jit(solution)/shard_map/all_gather | solution.py:80
  53.3 1.7 %fusion.6 = bf16[22,2,8,128]{3,2,1,0:T(8,128)(2,1)S(1)} fusion(bf16[2304,256]{1,0:T(8,128)(2,1)} %all-gather.2.cloned.1.call-done, bf16[1,176,2304]{2,1,0:T(8,128)(2,1)S(1)} %copy-done), kind=kOutput, calls=%fused_computation.21 | convolution fusion | flops 207663104 | bytes 2080768 | tf_op jit(solution)/shard_map/dot_general | solution.py:78
  55.0 6.3 %all_gather.11 = bf16[704,2,128]{2,0,1:T(8,128)(2,1)S(1)} all-gather(bf16[176,2,128]{2,0,1:T(8,128)(2,1)S(1)} %bitcast.73), channel_id=1, replica_groups=mesh['sp'=4,'dp'=8] {'sp'}, dimensions={0}, use_global_device_ids=true | all-gather | bytes 450560 | tf_op jit(solution)/shard_map/all_gather | solution.py:96
  61.3 13.4 %while.10 = (s32[]{:T(128)}, bf16[11,64,1,512]{3,1,2,0:T(8,128)(2,1)S(1)}, bf16[11,64,1,4,128]{4,3,1,0,2:T(4,128)(2,1)S(1)}, bf16[704,1,128]{2,0,1:T(8,128)(2,1)...) while((s32[]{:T(128)}, bf16[11,64,1,512]{3,1,2,0:T(8,128)(2,1)S(1)}, ...), condition=%wide.region_5.6_spmd, body=%wide.region_2.5_spmd.sunk | while | flops 93568512 | bytes 3183693 | solution.py:67
  63.2 0.4 fusion.22
  74.7 0.5 broadcast.195
  75.2 1.2 %reduce.2 = bf16[704,512]{1,0:T(8,128)(2,1)S(1)} reduce(bf16[704,1,512]{2,0,1:T(8,128)(2,1)S(1)} %bitcast.72, bf16[]{:T(256)} %broadcast.195), dimensions={1}, to_apply=%copy.43.reduce_sub_computation | reduce | bytes 1441794 | tf_op jit(solution)/shard_map/reshape | solution.py:67
  76.4 0.6 reshape.235
  77.0 13.3 %all_to_all.30 = bf16[4,2,45056]{2,1,0:T(2,128)(2,1)S(1)} all-to-all(bf16[4,2,45056]{2,1,0:T(2,128)(2,1)S(1)} %reshape.235), channel_id=1, replica_groups=mesh['sp'=4,'dp'=8] {'sp'}, dimensions={0} | all-to-all | bytes 1441792 | tf_op jit(solution)/shard_map/all_to_all | solution.py:103
  90.3 0.7 reshape.236
  91.2 0.6 copy.44
  91.8 1.4 %reshape.230 = bf16[1,176,2048]{2,1,0:T(8,128)(2,1)} reshape(bf16[176,4,1,512]{3,1,0,2:T(4,128)(2,1)S(1)} %copy.44) | data formatting | bytes 1441792 | tf_op jit(solution)/shard_map/reshape | solution.py:104
  (104 shorter events, 14.6 us)
Async XLA Ops:
  6.5 46.8 %copy-start = (bf16[1,176,2304]{2,1,0:T(8,128)(2,1)S(1)}, bf16[1,176,2304]{2,1,0:T(8,128)(2,1)}, u32[]{:S(2)}) copy-start(bf16[1,176,2304]{2,1,0:T(8,128)(2,1)} %param.10) | copy-start | bytes 2433028
  6.5 46.8 %all-gather.2.cloned.1.call-start = ((), (), s32[]{:S(2)}) async-start(), calls=%async_computation.2 | async-start | bytes 1327104 | tf_op jit(solution)/shard_map/all_gather | solution.py:80
  8.8 1.4 %copy-start.2 = (f32[128]{0:T(128)S(1)}, f32[128]{0:T(128)}, u32[]{:S(2)}) copy-start(f32[128]{0:T(128)} %param.12) | copy-start | bytes 1540
  13.1 5.4 %copy-start.1 = (bf16[1,176,256]{2,1,0:T(8,128)(2,1)S(1)}, bf16[1,176,256]{2,1,0:T(8,128)(2,1)}, u32[]{:S(2)}) copy-start(bf16[1,176,256]{2,1,0:T(8,128)(2,1)} %param.9) | copy-start | bytes 270340
  14.1 4.8 %copy-start.3 = (f32[128]{0:T(128)S(1)}, f32[128]{0:T(128)}, u32[]{:S(2)}) copy-start(f32[128]{0:T(128)} %param.13) | copy-start | bytes 1540
  14.1 18.5 %all-to-all-start = ((bf16[176,4,512]{2,0,1:T(8,128)(2,1)}), bf16[176,4,512]{2,0,1:T(8,128)(2,1)S(1)}, u32[]{:S(2)}, u32[]{:S(2)}) async-start(bf16[176,4,512]{2,0,1:T(8,128)(2,1)} %copy.37), calls=%async_computation | async-start | bytes 1441792 | tf_op jit(solution)/shard_map/all_to_all | solution.py:93
Sparse Core Ops, SparseCore 0:
  9.5 43.7 all-gather.1
where the time goes:
time: 100 us
  blocking collectives  31.4 us (31%)
  waiting for transfers between devices  21.3 us (21%)
  between operations  13.6 us (14%)
  other arithmetic  11 us (11%)
  matrix products  10 us (10%)
  local copies, waits for them, and re-layouts  7.71 us (8%)
  starting transfers between devices  4.4 us (4%)
    all_gather x1, waiting for transfers between devices, per_device(): lax.all_gather(w_value, 'dp', axis=0, tiled=True)  20.6 us
    all_to_all x1, blocking collectives, per_device(): lax.all_to_all(attended, 'sp', split_axis=0, concat_axis=1, tiled=True)  13.3 us
    all_gather x1, blocking collectives, per_device(): lax.all_gather(key_rot, 'sp', axis=0, tiled=True)  11.8 us
    all_gather x1, blocking collectives, per_device(): lax.all_gather(values, 'sp', axis=0, tiled=True)  6.26 us
    dot_general x11, matrix products, one_block(): jnp.einsum('naqk,knd->qnad', probability, value_heads, preferred_element_...  4.43 us
    all_to_all x1, starting transfers between devices, per_device(): lax.all_to_all(query_grouped, 'sp', split_axis=1, concat_axis=0, tiled=True)  4.4 us
    dot_general x11, matrix products, one_block(): jnp.einsum('qnad,knd->naqk', query_block, key_heads, preferred_element_ty...  3.96 us
    reduce_sum x11, other arithmetic, one_block(): jnp.sum(weights, axis=-1, keepdims=True)  3.07 us
  transfers between devices with their start and end apart: 2, of which 1 were waited for; matrix products, arithmetic and copies ran while one was open for 9% of the time, Pallas kernels for 0%

commit v1 on v0

--- a/solution.py
+++ b/solution.py
@@ -100,7 +100,10 @@
     key_local = lax.dynamic_slice_in_dim(key_all, kv_start, kv_count, 1)
     value_local = lax.dynamic_slice_in_dim(value_all, kv_start, kv_count, 1)
     attended = attend(query_local, key_local, value_local)
-    returned = lax.all_to_all(attended, "sp", split_axis=0, concat_axis=1, tiled=True)
+    returned = jnp.concatenate(
+        lax.all_to_all(jnp.stack(jnp.split(attended, lax.axis_size("sp"), axis=0)), "sp", 0, 0),
+        axis=1,
+    )
     return returned.reshape(1, tok_rows, QH * HD)
 
 

time: 100 us -> 97.3 us (0.973)
  local copies, waits for them, and re-layouts: 7.71 us -> 5.79 us
  other arithmetic: 11 us -> 9.92 us
    unnamed x12 -> x9, local copies, waits for them, and re-layouts: 1.73 us -> 0.28 us
    another operation x0 -> x2, local copies, waits for them, and re-layouts: none -> 1.44 us  [the longest x1 1.39 us: per_device(): return returned.reshape(1, tok_rows, QH * HD)]
    reshape x2 -> x1, local copies, waits for them, and re-layouts: 1.9 us -> 0.56 us  [per_device(): jnp.concatenate(lax.all_to_all(jnp.stack(jnp.split(attended, lax.axis_siz...]
    reshape x1 -> x0, other arithmetic: 1.19 us -> none  [attend(): return lax.map(one_block, blocked).reshape(length, item_count, joined)]
where the time goes in v1:
time: 97.3 us; the launch traced here: 97 us
  blocking collectives  31.4 us (32%)
  waiting for transfers between devices  21.3 us (22%)
  between operations  13.6 us (14%)
  matrix products  10 us (10%)
  other arithmetic  9.92 us (10%)
  local copies, waits for them, and re-layouts  5.79 us (6%)
  starting transfers between devices  4.4 us (5%)
    all_gather x1, waiting for transfers between devices, per_device(): lax.all_gather(w_value, 'dp', axis=0, tiled=True)  20.6 us
    all_to_all x1, blocking collectives, per_device(): lax.all_to_all(jnp.stack(jnp.split(attended, lax.axis_size('sp'), axis=0)...  13.3 us
    all_gather x1, blocking collectives, per_device(): lax.all_gather(key_rot, 'sp', axis=0, tiled=True)  11.8 us
    all_gather x1, blocking collectives, per_device(): lax.all_gather(values, 'sp', axis=0, tiled=True)  6.26 us
    dot_general x11, matrix products, one_block(): jnp.einsum('naqk,knd->qnad', probability, value_heads, preferred_element_...  4.43 us
    all_to_all x1, starting transfers between devices, per_device(): lax.all_to_all(query_grouped, 'sp', split_axis=1, concat_axis=0, tiled=True)  4.4 us
    dot_general x11, matrix products, one_block(): jnp.einsum('qnad,knd->naqk', query_block, key_heads, preferred_element_ty...  3.96 us
    reduce_sum x11, other arithmetic, one_block(): jnp.sum(weights, axis=-1, keepdims=True)  3.07 us
  transfers between devices with their start and end apart: 2, of which 1 were waited for; matrix products, arithmetic and copies ran while one was open for 9% of the time, Pallas kernels for 0%

profile of v1, /device:TPU:0, one launch (start us, length us, event | category | flops | bytes accessed | tf_op | source)
XLA Modules:
  0.0 97.0 jit_solution(7012689947114905107)
XLA Ops:
  6.5 0.7 all-gather.2.cloned.1.call-update
  7.3 1.3 %convert_bitcast_fusion = f32[22,8,16,128]{3,1,2,0:T(8,128)S(1)} fusion(bf16[1,176,2048]{2,1,0:T(8,128)(2,1)} %param.8), kind=kLoop, calls=%fused_computation.13 | loop fusion | flops 360448 | bytes 2162688
  8.8 0.4 multiply_reduce_fusion
  9.4 0.7 multiply_cosine_fusion.1
  10.2 0.4 multiply_multiply_fusion
  10.6 1.2 %subtract_convert_fusion.1 = (bf16[176,16,32]{2,1,0:T(8,128)(2,1)S(1)}, bf16[176,16,32]{2,1,0:T(8,128)(2,1)S(1)}, bf16[176,16,32]{2,1,0:T(8,128)(2,1)S(1)}, bf16[176,16,32]{2,1,0:T(8,128)(2,1)S(1)}) fusion(f32[176,16,128]{2,1,0:T(8,128)S(1)} %multiply_multiply_fusion, f32[176,32]{1,0:T(8,128)S(1)} %get-tuple-element.87, f32[176,32]{1,0:T(8,128)S(1)} %get-tuple-element.86, ...), kind=kLoop, calls=%fused_computation.17 | loop fusion | flops 1441792 | bytes 2252800 | tf_op jit(solution)/shard_map/convert.6
  11.8 0.9 pad_maximum_fusion
  13.1 1.0 %copy.38 = bf16[176,4,512]{2,0,1:T(8,128)(2,1)} copy(bf16[176,4,512]{2,1,0:T(4,128)(2,1)S(1)} %convert_element_type.64) | data formatting | bytes 1441792 | tf_op jit(solution)/shard_map/convert_element_type | solution.py:89
  14.1 4.4 %all-to-all-start = ((bf16[176,4,512]{2,0,1:T(8,128)(2,1)}), bf16[176,4,512]{2,0,1:T(8,128)(2,1)S(1)}, u32[]{:S(2)}, u32[]{:S(2)}) async-start(bf16[176,4,512]{2,0,1:T(8,128)(2,1)} %copy.38), calls=%async_computation | async-start | bytes 1441792 | tf_op jit(solution)/shard_map/all_to_all | solution.py:93
  19.1 0.6 subtract_convert_fusion.3
  19.8 0.6 pad_maximum_fusion.2
  20.3 11.8 %all_gather.9 = bf16[704,2,128]{2,1,0:T(2,128)(2,1)S(1)} all-gather(bf16[176,2,128]{2,1,0:T(2,128)(2,1)S(1)} %pad_maximum_fusion.2), channel_id=1, replica_groups=mesh['sp'=4,'dp'=8] {'sp'}, dimensions={0}, use_global_device_ids=true | all-gather | bytes 450560 | tf_op jit(solution)/shard_map/all_gather | solution.py:95
  32.8 20.6 %all-gather.2.cloned.1.call-done = bf16[2304,256]{1,0:T(8,128)(2,1)} async-done(((bf16[288,256]{1,0:T(8,128)(2,1)}), bf16[2304,256]{1,0:T(8,128)(2,1)}) %all-gather.2.cloned.1.call-update) | async-done | bytes 1179664 | tf_op jit(solution)/shard_map/all_gather | solution.py:80
  53.3 1.7 %fusion.6 = bf16[22,2,8,128]{3,2,1,0:T(8,128)(2,1)S(1)} fusion(bf16[2304,256]{1,0:T(8,128)(2,1)} %all-gather.2.cloned.1.call-done, bf16[1,176,2304]{2,1,0:T(8,128)(2,1)S(1)} %copy-done), kind=kOutput, calls=%fused_computation.21 | convolution fusion | flops 207663104 | bytes 2080768 | tf_op jit(solution)/shard_map/dot_general | solution.py:78
  55.0 6.3 %all_gather.11 = bf16[704,2,128]{2,0,1:T(8,128)(2,1)S(1)} all-gather(bf16[176,2,128]{2,0,1:T(8,128)(2,1)S(1)} %bitcast.79), channel_id=1, replica_groups=mesh['sp'=4,'dp'=8] {'sp'}, dimensions={0}, use_global_device_ids=true | all-gather | bytes 450560 | tf_op jit(solution)/shard_map/all_gather | solution.py:96
  61.3 13.4 %while.10 = (s32[]{:T(128)}, bf16[11,64,1,512]{3,1,2,0:T(8,128)(2,1)S(1)}, bf16[11,64,1,4,128]{4,3,1,0,2:T(4,128)(2,1)S(1)}, bf16[704,1,128]{2,0,1:T(8,128)(2,1)...) while((s32[]{:T(128)}, bf16[11,64,1,512]{3,1,2,0:T(8,128)(2,1)S(1)}, ...), condition=%wide.region_5.6_spmd, body=%wide.region_2.5_spmd.sunk | while | flops 93568512 | bytes 3183693 | solution.py:67
  63.2 0.4 fusion.22
  64.4 0.4 fusion.22
  66.9 0.4 fusion.22
  68.1 0.4 fusion.22
  70.5 0.4 fusion.22
  74.9 13.3 %all_to_all.20 = bf16[4,176,1,512]{3,1,2,0:T(8,128)(2,1)S(1)} all-to-all(bf16[4,176,1,512]{3,1,2,0:T(8,128)(2,1)S(1)} %pad_maximum_fusion.1), channel_id=1, replica_groups=mesh['sp'=4,'dp'=8] {'sp'}, dimensions={0} | all-to-all | bytes 1441792 | tf_op jit(solution)/shard_map/all_to_all | solution.py:104
  88.2 0.6 copy.44
  88.8 1.4 %reshape_reshape.3 = bf16[1,176,2048]{2,1,0:T(8,128)(2,1)} reshape(bf16[176,4,1,512]{3,1,0,2:T(4,128)(2,1)S(1)} %copy.44) | data formatting | bytes 1441792 | tf_op jit(solution)/shard_map/reshape;reshape | solution.py:107
  (101 shorter events, 13.0 us)
Async XLA Ops:
  6.5 46.8 %copy-start = (bf16[1,176,2304]{2,1,0:T(8,128)(2,1)S(1)}, bf16[1,176,2304]{2,1,0:T(8,128)(2,1)}, u32[]{:S(2)}) copy-start(bf16[1,176,2304]{2,1,0:T(8,128)(2,1)} %param.10) | copy-start | bytes 2433028
  6.5 46.8 %all-gather.2.cloned.1.call-start = ((), (), s32[]{:S(2)}) async-start(), calls=%async_computation.2 | async-start | bytes 1327104 | tf_op jit(solution)/shard_map/all_gather | solution.py:80
  8.8 1.4 %copy-start.2 = (f32[128]{0:T(128)S(1)}, f32[128]{0:T(128)}, u32[]{:S(2)}) copy-start(f32[128]{0:T(128)} %param.12) | copy-start | bytes 1540
  13.1 5.4 %copy-start.1 = (bf16[1,176,256]{2,1,0:T(8,128)(2,1)S(1)}, bf16[1,176,256]{2,1,0:T(8,128)(2,1)}, u32[]{:S(2)}) copy-start(bf16[1,176,256]{2,1,0:T(8,128)(2,1)} %param.9) | copy-start | bytes 270340
  14.1 4.8 %copy-start.3 = (f32[128]{0:T(128)S(1)}, f32[128]{0:T(128)}, u32[]{:S(2)}) copy-start(f32[128]{0:T(128)} %param.13) | copy-start | bytes 1540
  14.1 18.5 %all-to-all-start = ((bf16[176,4,512]{2,0,1:T(8,128)(2,1)}), bf16[176,4,512]{2,0,1:T(8,128)(2,1)S(1)}, u32[]{:S(2)}, u32[]{:S(2)}) async-start(bf16[176,4,512]{2,0,1:T(8,128)(2,1)} %copy.38), calls=%async_computation | async-start | bytes 1441792 | tf_op jit(solution)/shard_map/all_to_all | solution.py:93
Sparse Core Ops, SparseCore 0:
  9.5 43.7 all-gather.1
